TPU v7x, 32 devices: a whole 2x2x4 slice. The times are simulated.
32 devices in a mesh: rep: 4 (over z), fs: 4 (over y, x), tp: 2 (over core).
Axes of the slice: x: 2, y: 2, z: 4, core: 2. Of those that a mesh axis runs over, the one named last changes fastest.
Arguments:
- inputs: bfloat16 [4, 1024, 1024], P('rep', ('fs', 'tp')), may hold values from -6 to 6
- up_pre: bfloat16 [4, 1024, 2816], P('rep', None, ('fs', 'tp')), may hold values from -6 to 6
- gate_pre: bfloat16 [4, 1024, 2816], P('rep', None, ('fs', 'tp')), may hold values from -6 to 6
- cotangent: bfloat16 [4, 1024, 1024], P('rep', ('fs', 'tp')), may hold values from -6 to 6
- w_up: float32 [1024, 2816], P(None, ('fs', 'tp')), may hold values from -0.1875 to 0.1875
- w_gate: float32 [1024, 2816], P(None, ('fs', 'tp')), may hold values from -0.1875 to 0.1875
- w_down: float32 [2816, 1024], P(('fs', 'tp')), may hold values from -0.109375 to 0.109375
- conv_weight: float32 [3, 2816], P(None, ('fs', 'tp')), may hold values from -3.5 to 3.5
- conv_bias: float32 [2816], P(('fs', 'tp')), may hold values from -3 to 3
Outputs:
- grad_inputs: bfloat16 [4, 1024, 1024], P('rep', ('fs', 'tp'))
- grad_up: float32 [1024, 2816], P(None, ('fs', 'tp'))
- grad_gate: float32 [1024, 2816], P(None, ('fs', 'tp'))
- grad_down: float32 [2816, 1024], P(('fs', 'tp'))
- grad_conv_weight: float32 [3, 2816], P(None, ('fs', 'tp'))
- grad_conv_bias: float32 [2816], P(('fs', 'tp'))
All inputs are finite; a program needn't handle non-finite values.
Results may differ from a plain program's by a relative error of at most 0.0085.
Values may be sent and summed in bfloat16 or wider, within the bound.
A program may use at most 64 MiB of HBM per device.

v0:
```python
import jax
import jax.numpy as jnp
from jax import lax
from jax.sharding import PartitionSpec as P


def summed_rows(product, width, axis):
    everything = product(jnp.int32(0), lax.axis_size(axis) * width)
    own = lax.psum_scatter(everything, axis, scatter_dimension=0, tiled=True)
    return own


def taken_in(value, axis, dim, take_in, carry):
    whole = jax.tree.map(lambda part: lax.all_gather(part, axis, axis=dim, tiled=True), value)
    return take_in(carry, whole, jnp.int32(0))


def conv_forward(up_rows, conv_weight, conv_bias):
    length = up_rows.shape[0]
    tap_count = conv_weight.shape[0]
    padded = jnp.pad(up_rows, ((tap_count - 1, 0), (0, 0)))
    result = conv_bias + jnp.zeros_like(up_rows)
    for tap_index in range(tap_count):
        begin = tap_count - 1 - tap_index
        result = result + conv_weight[tap_index] * padded[begin : begin + length]
    return result


def conv_back(d_conv, up_rows, conv_weight):
    length = up_rows.shape[0]
    tap_count = conv_weight.shape[0]
    padded_grad = jnp.pad(d_conv, ((0, tap_count - 1), (0, 0)))
    padded_up = jnp.pad(up_rows, ((tap_count - 1, 0), (0, 0)))
    d_up = jnp.zeros_like(d_conv)
    tap_grads = []
    for tap_index in range(tap_count):
        d_up = d_up + conv_weight[tap_index] * padded_grad[tap_index : tap_index + length]
        begin = tap_count - 1 - tap_index
        tap_grads.append(jnp.sum(d_conv * padded_up[begin : begin + length], axis=0))
    return (d_up, jnp.stack(tap_grads), jnp.sum(d_conv, axis=0))


def on_device(inputs, up_pre, gate_pre, cotangent, w_up, w_gate, w_down, conv_weight, conv_bias):
    seq_len = up_pre.shape[1]
    factor = float(lax.axis_size("rep") * seq_len) ** (-0.5)
    up_mat = w_up.astype(jnp.bfloat16)
    gate_mat = w_gate.astype(jnp.bfloat16)
    down_mat = w_down.astype(jnp.bfloat16)
    up_rows = up_pre[0].astype(jnp.float32)
    gate_rows = gate_pre[0].astype(jnp.float32)
    convolved = conv_forward(up_rows, conv_weight, conv_bias)
    activated, pullback = jax.vjp(jax.nn.gelu, convolved)
    hidden = (activated * gate_rows).astype(jnp.bfloat16)
    whole_cot = lax.all_gather(cotangent[0], ("fs", "tp"), axis=0, tiled=True)
    d_hidden = jnp.dot(whole_cot, down_mat.T, preferred_element_type=jnp.float32).astype(
        jnp.bfloat16
    )
    d_hidden_f = d_hidden.astype(jnp.float32)
    d_gate = (d_hidden_f * activated).astype(jnp.bfloat16)
    d_conv = pullback(d_hidden_f * gate_rows)[0]
    d_up_f, tap_grad, bias_grad = conv_back(d_conv, up_rows, conv_weight)
    d_up = d_up_f.astype(jnp.bfloat16)
    local_rows = inputs.shape[1]

    def input_part():

        def rows_term(offset, row_count):
            rows_up = lax.dynamic_slice_in_dim(d_up, offset, row_count, 0)
            rows_gate = lax.dynamic_slice_in_dim(d_gate, offset, row_count, 0)
            return jnp.dot(rows_up, up_mat.T, preferred_element_type=jnp.float32) + jnp.dot(
                rows_gate, gate_mat.T, preferred_element_type=jnp.float32
            )

        summed = summed_rows(rows_term, local_rows, ("fs", "tp"))
        return summed.astype(jnp.bfloat16)[None]

    def weight_part():
        g_down = jnp.dot(hidden.T, whole_cot, preferred_element_type=jnp.float32) * factor

        def add_rows(running, gathered, offset):
            rows_up = lax.dynamic_slice_in_dim(d_up, offset, gathered.shape[0], 0)
            rows_gate = lax.dynamic_slice_in_dim(d_gate, offset, gathered.shape[0], 0)
            numbers = (((0,), (0,)), ((), ()))
            return (
                running[0]
                + lax.dot_general(gathered, rows_up, numbers, preferred_element_type=jnp.float32),
                running[1]
                + lax.dot_general(gathered, rows_gate, numbers, preferred_element_type=jnp.float32),
            )

        blank_grad = jnp.zeros((inputs.shape[2], up_pre.shape[2]), jnp.float32)
        g_up, g_gate = taken_in(inputs[0], ("fs", "tp"), 0, add_rows, (blank_grad, blank_grad))
        g_up = g_up * factor
        g_gate = g_gate * factor
        g_taps = tap_grad * factor
        g_bias = bias_grad * factor
        g_down = lax.psum(g_down, "rep")
        g_up, g_gate = lax.psum((g_up, g_gate), "rep")
        g_taps, g_bias = lax.psum((g_taps, g_bias), "rep")
        return (g_up, g_gate, g_down, g_taps, g_bias)

    grad_inputs = input_part()
    weight_grads = weight_part()
    return (
        grad_inputs,
        weight_grads[0],
        weight_grads[1],
        weight_grads[2],
        weight_grads[3],
        weight_grads[4],
    )


def solution(mesh):
    return jax.shard_map(
        on_device,
        mesh=mesh,
        in_specs=(
            P("rep", ("fs", "tp"), None),
            P("rep", None, ("fs", "tp")),
            P("rep", None, ("fs", "tp")),
            P("rep", ("fs", "tp"), None),
            P(None, ("fs", "tp")),
            P(None, ("fs", "tp")),
            P(("fs", "tp"), None),
            P(None, ("fs", "tp")),
            P(("fs", "tp")),
        ),
        out_specs=(
            P("rep", ("fs", "tp"), None),
            P(None, ("fs", "tp")),
            P(None, ("fs", "tp")),
            P(("fs", "tp"), None),
            P(None, ("fs", "tp")),
            P(("fs", "tp")),
        ),
        check_vma=False,
    )
```

profile of v0, /device:TPU:0, one launch (start us, length us, event | category | flops | bytes accessed | tf_op | source)
XLA Modules:
  0.0 297.6 jit_solution(11588245199680852558)
XLA Ops:
  7.2 0.7 all-gather.5.cloned.1.call-update
  8.0 0.7 all-gather.7.cloned.1.call-update
  8.7 0.8 slice_reduce_fusion.2
  9.5 1.3 bitcast_convert_fusion
  10.8 29.4 %all-gather.5.cloned.1.call-done = bf16[1,1024,1024]{2,1,0:T(8,128)(2,1)} async-done(((bf16[1,128,1024]{2,1,0:T(8,128)(2,1)}), bf16[1,1024,1024]{2,1,0:T(8,128)(2,1)}) %all-gather.5.cloned.1.call-update) | async-done | bytes 2097168 | tf_op jit(solution)/shard_map/all_gather | solution.py:54
  40.2 4.8 %multiply_reduce_fusion.1 = (f32[352]{0:T(512)S(1)}, f32[352]{0:T(512)S(1)}, f32[352]{0:T(512)S(1)}, f32[352]{0:T(512)S(1)}, f32[1024,352]{0,1:T(8,128)S(1)}, /*...) fusion(f32[1024,352]{0,1:T(8,128)S(1)} %bitcast_convert_fusion, bf16[1,1024,352]{1,2,0:T(8,128)(2,1)} %param.10, ...), kind=kOutput, calls=%fused_computation.37 | convolution fusion | flops 751892992 | bytes 10038272 | tf_op jit(solution)/shard_map/dot_general | solution.py:55
  45.0 1.1 fusion.26
  46.1 0.5 copy-done
  46.6 1.3 fusion.42
  47.9 0.0 copy-done.3
  48.0 3.6 %convolution_add_fusion = f32[1024,1024]{1,0:T(8,128)} fusion(f32[1024,1024]{1,0:T(8,128)S(1)} %fusion.42, f32[1024,352]{0,1:T(8,128)S(1)} %copy-done.3, bf16[1024,352]{0,1:T(8,128)(2,1)S(1)} %get-tuple-element.20, f32[1024,352]{0,1:T(8,128)S(1)} %get-tuple-element.19), kind=kOutput, calls=%fused_computation | convolution fusion | flops 743571456 | bytes 11993088 | tf_op jit(solution)/shard_map/dot_general | solution.py:70
  51.6 0.0 all-reduce.6.cloned.1.call-start
  51.7 18.0 %all-gather.7.cloned.1.call-done = bf16[1,1024,1024]{2,1,0:T(8,128)(2,1)} async-done(((bf16[1,128,1024]{2,1,0:T(8,128)(2,1)}), bf16[1,1024,1024]{2,1,0:T(8,128)(2,1)}) %all-gather.7.cloned.1.call-update) | async-done | bytes 2097168 | tf_op jit(solution)/shard_map/all_gather | solution.py:14
  69.7 3.8 %fusion.20 = f32[1024,352]{0,1:T(8,128)} fusion(bf16[1024,352]{0,1:T(8,128)(2,1)S(1)} %fusion.26, bf16[1,1024,1024]{2,1,0:T(8,128)(2,1)} %all-gather.7.cloned.1.call-done), kind=kOutput, calls=%fused_computation.22 | convolution fusion | flops 738557952 | bytes 4259840 | tf_op jit(solution)/shard_map/dot_general | solution.py:86
  73.5 2.3 fusion.17
  75.7 2.3 fusion.8
  78.1 12.4 %all-reduce.2 = (f32[3,352]{1,0:T(4,128)}, f32[352]{0:T(512)}) all-reduce(f32[3,352]{1,0:T(4,128)S(1)} %maximum_multiply_fusion, f32[352]{0:T(512)S(1)} %broadcast_multiply_fusion), channel_id=1, replica_groups=mesh['rep'=4,'fs'=4,'tp'=2] {'rep'}, use_global_device_ids=true, to_apply=%region_7.8 | all-reduce | flops 1408 | bytes 11264 | tf_op jit(solution)/shard_map/psum | solution.py:99
  90.5 33.5 %reduce-scatter.2.cloned.1.call-done = f32[128,1024]{1,0:T(8,128)} async-done(((f32[1024,1024]{1,0:T(8,128)}), f32[128,1024]{1,0:T(8,128)}) %reduce-scatter.2.cloned.1.call-update) | async-done | bytes 524304 | tf_op jit(solution)/shard_map/reduce_scatter | solution.py:9
  124.1 1.8 convert_bitcast_fusion
  125.8 159.5 %all-reduce.6.cloned.1.call-done = (f32[1024,352]{0,1:T(8,128)}, f32[1024,352]{0,1:T(8,128)}, f32[352,1024]{1,0:T(8,128)}) async-done(((f32[1024,352]{0,1:T(8,128)}, f32[1024,352]{0,1:T(8,128)}, f32[352,1024]{1,0:T(8,128)}), (f32[1024,352]{0,1:T(8,128)}, f32[1024,352]{0,1:T(8,128)}, f32[352,1024]{1,0:T(8,128)})) %all-reduce.6.cloned.1.call-update) | async-done | bytes 4325392 | tf_op jit(solution)/shard_map/psum | solution.py:98
  285.3 2.7 copy.18
  288.1 1.1 copy.19
  289.2 0.8 copy-done.1
  290.0 1.1 copy.20
  (27 shorter events, 0.2 us)
Async XLA Ops:
  7.2 33.1 %copy-start.9 = (f32[352]{0:T(512)S(1)}, f32[352]{0:T(512)}, u32[]{:S(2)}) copy-start(f32[352]{0:T(512)} %param.17) | copy-start | bytes 4228
  7.2 33.1 %all-gather.5.cloned.1.call-start = ((), (), s32[]{:S(2)}) async-start(), calls=%async_computation.2 | async-start | bytes 2359296 | tf_op jit(solution)/shard_map/all_gather | solution.py:54
  7.9 61.8 %all-gather.7.cloned.1.call-start = ((), (), s32[]{:S(2)}) async-start(), calls=%async_computation.3 | async-start | bytes 2359296 | tf_op jit(solution)/shard_map/all_gather | solution.py:14
  8.7 115.4 %reduce-scatter.2.cloned.1.call-start = ((), (), s32[]{:S(2)}) async-start(), calls=%async_computation.1 | async-start | bytes 4718592 | tf_op jit(solution)/shard_map/reduce_scatter | solution.py:9
  45.0 2.9 copy-start.4
  45.0 1.6 copy-start
  46.6 1.4 copy-start.3
  51.6 21.9 %copy-start.5 = (bf16[1024,352]{0,1:T(8,128)(2,1)S(1)}, bf16[1024,352]{0,1:T(8,128)(2,1)}, u32[]{:S(2)}) copy-start(bf16[1024,352]{0,1:T(8,128)(2,1)} %copy-done.4) | copy-start | bytes 2162692
  51.6 233.7 %all-reduce.6.cloned.1.call-start = ((), (), s32[]{:S(2)}) async-start(), calls=%async_computation.4 | async-start | bytes 8650752 | tf_op jit(solution)/shard_map/psum | solution.py:98
  69.7 3.8 %copy-start.7 = (bf16[1,1024,1024]{2,1,0:T(8,128)(2,1)S(1)}, bf16[1,1024,1024]{2,1,0:T(8,128)(2,1)}, u32[]{:S(2)}) copy-start(bf16[1,1024,1024]{2,1,0:T(8,128)(2,1)} %all-gather.7.cloned.1.call-done) | copy-start | bytes 6291460
  73.5 2.3 copy-start.6
  73.5 2.3 copy-start.8
  285.3 2.7 copy-start.2
  288.1 1.9 copy-start.1
Sparse Core Ops, SparseCore 0:
  9.9 30.3 all-gather.4
  42.1 27.5 all-gather.6
  73.1 50.9 reduce-scatter.1
  127.1 158.2 all-reduce.5
where the time goes:
time: 298 us
  waiting for transfers between devices  242 us (81%)
  matrix products  17.9 us (6%)
  between operations  13.9 us (5%)
  blocking collectives  12.4 us (4%)
  local copies, waits for them, and re-layouts  7.18 us (2%)
  other arithmetic  4.12 us (1%)
    psum x1, waiting for transfers between devices, weight_part(): g_up, g_gate = lax.psum((g_up, g_gate), 'rep')  160 us
    reduce_scatter x1, waiting for transfers between devices, summed_rows(): own = lax.psum_scatter(everything, axis, scatter_dimension=0, tiled=True)  33.5 us
    all_gather x1, waiting for transfers between devices, on_device(): whole_cot = lax.all_gather(cotangent[0], ('fs', 'tp'), axis=0, tiled=True)  29.4 us
    all_gather x1, waiting for transfers between devices, taken_in(): lax.all_gather(part, axis, axis=dim, tiled=True)  18 us
    psum x1, blocking collectives, weight_part(): g_taps, g_bias = lax.psum((g_taps, g_bias), 'rep')  12.4 us
    unnamed x23, local copies, waits for them, and re-layouts  6.34 us
  transfers between devices with their start and end apart: 4, of which 4 were waited for; matrix products, arithmetic and copies ran while one was open for 8% of the time, Pallas kernels for 0%

commit v1 on v0

v1 whole, which is shorter than its diff:
```python
import functools
import math

import jax
import jax.numpy as jnp
from jax import lax
from jax.experimental import pallas as pl
from jax.experimental.pallas import tpu as pltpu
from jax.sharding import PartitionSpec as P

MESH = pl.DeviceIdType.MESH
F32 = jnp.float32
BF16 = jnp.bfloat16
SLOPE = math.sqrt(2.0 / math.pi)
CUBIC = 0.044715
HALO = 8
WIDE = 512
CHUNK = 256
ROWS = 128


def kernel(
    sizes,
    cot_ref,
    in_ref,
    taps_ref,
    bias_ref,
    up_hbm,
    gate_hbm,
    wdown_hbm,
    wup_hbm,
    wgate_hbm,
    gi_ref,
    fin,
    conv_out,
    cot_all,
    in_all,
    up_raw,
    gate_raw,
    wdown_f,
    wup_f,
    wgate_f,
    up_pad,
    act,
    slope_gate,
    hid,
    dconv,
    dgate,
    dup,
    down_b,
    up_b,
    gate_b,
    part,
    stage,
    conv_all,
    pair_send,
    pair_recv,
    keep,
    ring_send,
    ring_recv,
    load_sem,
    ag_send,
    ag_recv,
    part_send,
    part_recv,
    fin_send,
    fin_recv,
    conv_send,
    conv_recv,
    pair_ssem,
    pair_rsem,
    ring_ssem,
    ring_rsem,
):
    n_rep, n_fs, n_tp = sizes
    me_r, me_f, me_c = lax.axis_index("rep"), lax.axis_index("fs"), lax.axis_index("tp")
    seq, width = cot_all.shape
    ff = hid.shape[1]
    block = cot_ref.shape[0]
    taps = taps_ref.shape[0]
    per_grad = width // CHUNK
    chunks = 3 * per_grad
    me_block = me_f * n_tp + me_c

    loads = [
        pltpu.make_async_copy(src, dst, load_sem.at[at])
        for at, (src, dst) in enumerate(
            (
                (up_hbm, up_raw),
                (gate_hbm, gate_raw),
                (wdown_hbm, wdown_f),
                (wup_hbm, wup_f),
                (wgate_hbm, wgate_f),
            )
        )
    ]
    for load in loads:
        load.start()

    def other(me, step, count):
        return lax.rem(me + step, count)

    barrier = pltpu.get_barrier_semaphore()
    for axis, me, count in (("rep", me_r, n_rep), ("fs", me_f, n_fs), ("tp", me_c, n_tp)):
        for step in range(1, count):
            pl.semaphore_signal(
                barrier, inc=1, device_id={axis: other(me, step, count)}, device_id_type=MESH
            )
    pl.semaphore_wait(barrier, n_rep + n_fs + n_tp - 3)

    def remote(src, dst, send, recv, target):
        return pltpu.make_async_remote_copy(
            src_ref=src,
            dst_ref=dst,
            send_sem=send,
            recv_sem=recv,
            device_id=target,
            device_id_type=MESH,
        )

    def rows_of(index):
        return pl.ds(pl.multiple_of(index * block, block), block)

    def gather_sends(which, own_ref, whole):
        own = rows_of(me_block)
        sent = []
        for step in range(1, n_fs):
            sent.append(
                remote(
                    own_ref,
                    whole.at[own],
                    ag_send.at[which, step],
                    ag_recv.at[which, me_block],
                    {"fs": other(me_f, step, n_fs)},
                )
            )
        for step in range(1, n_tp):
            sent.append(
                remote(
                    own_ref,
                    whole.at[own],
                    ag_send.at[which, n_fs * step],
                    ag_recv.at[which, me_block],
                    {"tp": other(me_c, step, n_tp)},
                )
            )
        for copy in sent:
            copy.start()
        whole[own, :] = own_ref[...]
        return sent

    def gather_finish(which, own_ref, whole):
        passed = []
        for step in range(1, n_fs):
            source = other(me_f, n_fs - step, n_fs) * n_tp + me_c
            here = whole.at[rows_of(source)]
            remote(
                own_ref, here, ag_send.at[which, 0], ag_recv.at[which, source], {"fs": me_f}
            ).wait_recv()
            for hop in range(1, n_tp):
                copy = remote(
                    here,
                    here,
                    ag_send.at[which, n_fs * hop + step],
                    ag_recv.at[which, source],
                    {"tp": other(me_c, hop, n_tp)},
                )
                copy.start()
                passed.append(copy)
        for step in range(n_fs):
            for hop in range(1, n_tp):
                source = other(me_f, n_fs - step, n_fs) * n_tp + other(me_c, hop, n_tp)
                here = whole.at[rows_of(source)]
                remote(
                    own_ref, here, ag_send.at[which, 0], ag_recv.at[which, source], {"fs": me_f}
                ).wait_recv()
        return passed

    pending = gather_sends(0, cot_ref, cot_all)

    bias = bias_ref[...]
    weight = [taps_ref[pl.ds(k, 1), :] for k in range(taps)]
    up_pad[pl.ds(0, HALO), :] = jnp.zeros((HALO, ff), F32)
    dconv[pl.ds(seq, HALO), :] = jnp.zeros((HALO, ff), F32)
    loads[0].wait()
    loads[1].wait()

    def forward(at, _):
        rows = pl.ds(pl.multiple_of(at * ROWS, ROWS), ROWS)
        low = pl.multiple_of(at * ROWS, ROWS)
        up_pad[pl.ds(pl.multiple_of(low + HALO, HALO), ROWS), :] = up_raw[rows, :].astype(F32)
        ext = up_pad[pl.ds(low, ROWS + HALO), :]
        total = bias + jnp.zeros((ROWS, ff), F32)
        for k in range(taps):
            total = total + weight[k] * ext[HALO - k : HALO - k + ROWS]
        square = total * total
        bend = jnp.tanh(SLOPE * total * (1.0 + CUBIC * square))
        half = 0.5 * (1.0 + bend)
        active = total * half
        slope = half + 0.5 * total * (1.0 - bend * bend) * (
            SLOPE * (1.0 + 3.0 * CUBIC * square)
        )
        gate = gate_raw[rows, :].astype(F32)
        act[rows, :] = active
        hid[rows, :] = (active * gate).astype(BF16)
        slope_gate[rows, :] = slope * gate
        return 0

    lax.fori_loop(0, seq // ROWS, forward, 0)
    loads[2].wait()
    down_b[...] = wdown_f[...].astype(BF16)
    loads[3].wait()
    loads[4].wait()
    up_b[...] = wup_f[...].astype(BF16)
    gate_b[...] = wgate_f[...].astype(BF16)

    pending += gather_finish(0, cot_ref, cot_all)
    pending += gather_sends(1, in_ref, in_all)

    def owner_of(j):
        return n_rep // 2 - 1 + j % 2

    def has_away(j):
        o = owner_of(j)
        return jnp.logical_or(
            jnp.logical_and(me_r < o, me_r > 0),
            jnp.logical_and(me_r > o, me_r < n_rep - 1),
        )

    def partial_copy(j):
        o = owner_of(j)
        side = jnp.where(me_r < o, 0, 1)
        toward = jnp.clip(jnp.where(me_r < o, me_r + 1, me_r - 1), 0, n_rep - 1)
        return remote(
            stage.at[j], part.at[side, j], part_send.at[j], part_recv.at[side, j], {"rep": toward}
        )

    def wait_part(side, j):
        remote(
            stage.at[j], part.at[side, j], part_send.at[j], part_recv.at[side, j], {"rep": me_r}
        ).wait_recv()

    def final_copy(j, way):
        target = jnp.clip(me_r + (1 if way else -1), 0, n_rep - 1)
        return remote(
            fin.at[j], fin.at[j], fin_send.at[way, j], fin_recv.at[j], {"rep": target}
        )

    def is_edge(j):
        return jnp.logical_and(me_r != owner_of(j), jnp.logical_not(has_away(j)))

    def start_edge(j):
        @pl.when(is_edge(j))
        def _():
            partial_copy(j).start()

    def advance(j):
        o = owner_of(j)
        for side in (0, 1):
            inner = (me_r < o) if side == 0 else (me_r > o)

            @pl.when(jnp.logical_and(inner, has_away(j)))
            def _(side=side):
                wait_part(side, j)
                stage[j] = (stage[j].astype(F32) + part[side, j].astype(F32)).astype(BF16)
                partial_copy(j).start()

        @pl.when(me_r == o)
        def _():
            total = stage[j].astype(F32)
            if o > 0:
                wait_part(0, j)
                total = total + part[0, j].astype(F32)
            if o < n_rep - 1:
                wait_part(1, j)
                total = total + part[1, j].astype(F32)
            fin[j] = total.astype(BF16)
            if o > 0:
                final_copy(j, 0).start()
            if o < n_rep - 1:
                final_copy(j, 1).start()

    def deliver(j):
        o = owner_of(j)

        @pl.when(me_r != o)
        def _():
            final_copy(j, 0).wait_recv()

        @pl.when(jnp.logical_and(me_r < o, me_r > 0))
        def _():
            final_copy(j, 0).start()

        @pl.when(jnp.logical_and(me_r > o, me_r < n_rep - 1))
        def _():
            final_copy(j, 1).start()

    over_rows = (((0,), (0,)), ((), ()))
    over_cols = (((1,), (1,)), ((), ()))

    def weight_grad(grad, left, right):
        for piece in range(width // WIDE):
            product = lax.dot_general(
                left[...],
                right[:, pl.ds(piece * WIDE, WIDE)],
                over_rows,
                preferred_element_type=F32,
            ).astype(BF16)
            for sub in range(WIDE // CHUNK):
                j = grad * per_grad + piece * (WIDE // CHUNK) + sub
                stage[j] = product[:, sub * CHUNK : (sub + 1) * CHUNK]
                start_edge(j)

    weight_grad(0, hid, cot_all)

    def backward(at, sums):
        low = pl.multiple_of(at * ROWS, ROWS)
        rows = pl.ds(low, ROWS)
        d_hidden = (
            lax.dot_general(cot_all[rows, :], down_b[...], over_cols, preferred_element_type=F32)
            .astype(BF16)
            .astype(F32)
        )
        dgate[rows, :] = (d_hidden * act[rows, :]).astype(BF16)
        d_conv = d_hidden * slope_gate[rows, :]
        dconv[rows, :] = d_conv
        ext = up_pad[pl.ds(low, ROWS + HALO), :]
        new = [
            sums[k]
            + jnp.sum(d_conv * ext[HALO - k : HALO - k + ROWS], axis=0, keepdims=True)
            for k in range(taps)
        ]
        return (*new, sums[taps] + jnp.sum(d_conv, axis=0, keepdims=True))

    sums = lax.fori_loop(
        0, seq // ROWS, backward, tuple(jnp.zeros((1, ff), F32) for _ in range(taps + 1))
    )
    conv_all[me_r] = jnp.zeros(conv_all.shape[1:], F32)
    for k in range(taps + 1):
        conv_all[me_r, pl.ds(k, 1), :] = sums[k]

    def spread(at, _):
        low = pl.multiple_of(at * ROWS, ROWS)
        ext = dconv[pl.ds(low, ROWS + HALO), :]
        total = weight[0] * ext[0:ROWS]
        for k in range(1, taps):
            total = total + weight[k] * ext[k : k + ROWS]
        dup[pl.ds(low, ROWS), :] = total.astype(BF16)
        return 0

    lax.fori_loop(0, seq // ROWS, spread, 0)

    for step in range(1, n_rep):
        copy = remote(
            conv_all.at[me_r],
            conv_all.at[me_r],
            conv_send.at[step],
            conv_recv.at[me_r],
            {"rep": other(me_r, step, n_rep)},
        )
        copy.start()
        pending.append(copy)

    advance(0)
    pending += gather_finish(1, in_ref, in_all)
    weight_grad(1, dup, in_all)
    advance(1)
    weight_grad(2, dgate, in_all)
    advance(2)

    def input_rows(core, store):
        left_up = jnp.concatenate(
            [dup[rows_of(f * n_tp + core), :] for f in range(n_fs)], axis=0
        )
        left_gate = jnp.concatenate(
            [dgate[rows_of(f * n_tp + core), :] for f in range(n_fs)], axis=0
        )
        for piece in range(width // WIDE):
            cols = pl.ds(piece * WIDE, WIDE)
            total = lax.dot_general(
                left_up, up_b[cols, :], over_cols, preferred_element_type=F32
            ) + lax.dot_general(
                left_gate, gate_b[cols, :], over_cols, preferred_element_type=F32
            )
            store(cols, total)

    for hop in range(1, n_tp):

        def store_pair(cols, total, hop=hop):
            pair_send[hop - 1, :, cols] = total.astype(BF16)

        input_rows(other(me_c, hop, n_tp), store_pair)
        copy = remote(
            pair_send.at[hop - 1],
            pair_recv.at[hop - 1],
            pair_ssem.at[hop - 1],
            pair_rsem.at[hop - 1],
            {"tp": other(me_c, hop, n_tp)},
        )
        copy.start()
        pending.append(copy)
    deliver(0)
    advance(3)

    def store_keep(cols, total):
        keep[:, cols] = total

    input_rows(me_c, store_keep)
    for hop in range(1, n_tp):
        remote(
            pair_send.at[hop - 1],
            pair_recv.at[hop - 1],
            pair_ssem.at[hop - 1],
            pair_rsem.at[hop - 1],
            {"tp": other(me_c, hop, n_tp)},
        ).wait_recv()
    for step in range(1, n_fs):
        target = other(me_f, step, n_fs)
        rows = rows_of(target)
        total = keep[rows, :]
        for hop in range(1, n_tp):
            total = total + pair_recv[hop - 1, rows, :].astype(F32)
        ring_send[step] = total.astype(BF16)
        copy = remote(
            ring_send.at[step],
            ring_recv.at[step],
            ring_ssem.at[step],
            ring_rsem.at[step],
            {"fs": target},
        )
        copy.start()
        pending.append(copy)
    deliver(1)
    for j in range(4, chunks):
        advance(j)
        deliver(j - 2)

    own = rows_of(me_f)
    total = keep[own, :]
    for hop in range(1, n_tp):
        total = total + pair_recv[hop - 1, own, :].astype(F32)
    for step in range(1, n_fs):
        remote(
            ring_send.at[step],
            ring_recv.at[step],
            ring_ssem.at[step],
            ring_rsem.at[step],
            {"fs": me_f},
        ).wait_recv()
        total = total + ring_recv[step].astype(F32)
    gi_ref[...] = total.astype(BF16)

    for step in range(1, n_rep):
        source = other(me_r, n_rep - step, n_rep)
        remote(
            conv_all.at[source],
            conv_all.at[source],
            conv_send.at[0],
            conv_recv.at[source],
            {"rep": me_r},
        ).wait_recv()
    total = conv_all[0]
    for at in range(1, n_rep):
        total = total + conv_all[at]
    conv_out[...] = total

    for j in range(chunks - 2, chunks):
        deliver(j)

    for copy in pending:
        copy.wait_send()
    for j in range(chunks):
        o = owner_of(j)

        @pl.when(me_r != o)
        def _():
            partial_copy(j).wait_send()

        @pl.when(jnp.logical_and(me_r <= o, me_r > 0))
        def _():
            final_copy(j, 0).wait_send()

        @pl.when(jnp.logical_and(me_r >= o, me_r < n_rep - 1))
        def _():
            final_copy(j, 1).wait_send()


def on_device(
    sizes, inputs, up_pre, gate_pre, cotangent, w_up, w_gate, w_down, conv_weight, conv_bias
):
    n_rep, n_fs, n_tp = sizes
    seq, ff = up_pre.shape[1:]
    block, width = inputs.shape[1:]
    taps = conv_weight.shape[0]
    factor = float(n_rep * seq) ** (-0.5)
    chunks = 3 * width // CHUNK
    devices = n_fs * n_tp
    vmem = pl.BlockSpec(memory_space=pltpu.VMEM)
    hbm = pl.BlockSpec(memory_space=pl.ANY)
    conv_rows = -(-(taps + 1) // 8) * 8
    dma = pltpu.SemaphoreType.DMA
    grad_inputs, fin, conv = pl.pallas_call(
        functools.partial(kernel, sizes),
        out_shape=(
            jax.ShapeDtypeStruct((block, width), BF16),
            jax.ShapeDtypeStruct((chunks, ff, CHUNK), BF16),
            jax.ShapeDtypeStruct((conv_rows, ff), F32),
        ),
        in_specs=[vmem] * 4 + [hbm] * 5,
        out_specs=(vmem, vmem, vmem),
        scratch_shapes=[
            pltpu.VMEM((seq, width), BF16),
            pltpu.VMEM((seq, width), BF16),
            pltpu.VMEM((seq, ff), BF16),
            pltpu.VMEM((seq, ff), BF16),
            pltpu.VMEM((ff, width), F32),
            pltpu.VMEM((width, ff), F32),
            pltpu.VMEM((width, ff), F32),
            pltpu.VMEM((seq + HALO, ff), F32),
            pltpu.VMEM((seq, ff), F32),
            pltpu.VMEM((seq, ff), F32),
            pltpu.VMEM((seq, ff), BF16),
            pltpu.VMEM((seq + HALO, ff), F32),
            pltpu.VMEM((seq, ff), BF16),
            pltpu.VMEM((seq, ff), BF16),
            pltpu.VMEM((ff, width), BF16),
            pltpu.VMEM((width, ff), BF16),
            pltpu.VMEM((width, ff), BF16),
            pltpu.VMEM((2, chunks, ff, CHUNK), BF16),
            pltpu.VMEM((chunks, ff, CHUNK), BF16),
            pltpu.VMEM((n_rep, conv_rows, ff), F32),
            pltpu.VMEM((n_tp - 1, n_fs * block, width), BF16),
            pltpu.VMEM((n_tp - 1, n_fs * block, width), BF16),
            pltpu.VMEM((n_fs * block, width), F32),
            pltpu.VMEM((n_fs, block, width), BF16),
            pltpu.VMEM((n_fs, block, width), BF16),
            dma((5,)),
            dma((2, n_fs * n_tp)),
            dma((2, devices)),
            dma((chunks,)),
            dma((2, chunks)),
            dma((2, chunks)),
            dma((chunks,)),
            dma((n_rep,)),
            dma((n_rep,)),
            dma((n_tp,)),
            dma((n_tp,)),
            dma((n_fs,)),
            dma((n_fs,)),
        ],
        compiler_params=pltpu.CompilerParams(
            collective_id=0, has_side_effects=True, vmem_limit_bytes=62 << 20
        ),
    )(
        cotangent[0],
        inputs[0],
        conv_weight,
        conv_bias[None],
        up_pre[0],
        gate_pre[0],
        w_down,
        w_up,
        w_gate,
    )
    per_grad = width // CHUNK
    parts = fin.reshape(3, per_grad, ff, CHUNK)
    g_down = parts[0].transpose(1, 0, 2).reshape(ff, width).astype(F32) * factor
    g_up = parts[1].transpose(0, 2, 1).reshape(width, ff).astype(F32) * factor
    g_gate = parts[2].transpose(0, 2, 1).reshape(width, ff).astype(F32) * factor
    conv = conv * factor
    return grad_inputs[None], g_up, g_gate, g_down, conv[:taps], conv[taps]


def solution(mesh):
    sizes = tuple(mesh.shape[axis] for axis in ("rep", "fs", "tp"))
    return jax.shard_map(
        functools.partial(on_device, sizes),
        mesh=mesh,
        in_specs=(
            P("rep", ("fs", "tp"), None),
            P("rep", None, ("fs", "tp")),
            P("rep", None, ("fs", "tp")),
            P("rep", ("fs", "tp"), None),
            P(None, ("fs", "tp")),
            P(None, ("fs", "tp")),
            P(("fs", "tp"), None),
            P(None, ("fs", "tp")),
            P(("fs", "tp")),
        ),
        out_specs=(
            P("rep", ("fs", "tp"), None),
            P(None, ("fs", "tp")),
            P(None, ("fs", "tp")),
            P(("fs", "tp"), None),
            P(None, ("fs", "tp")),
            P(("fs", "tp")),
        ),
        check_vma=False,
    )
```

time: 298 us -> 146 us (0.49)
  waiting for transfers between devices: 242 us -> 0 us
  Pallas kernels: 0 us -> 127 us
  matrix products: 17.9 us -> 0 us
  between operations: 13.9 us -> 0.67 us
  blocking collectives: 12.4 us -> 0 us
  local copies, waits for them, and re-layouts: 7.18 us -> 13.8 us
    psum x1 -> x0, waiting for transfers between devices: 160 us -> none  [weight_part(): g_up, g_gate = lax.psum((g_up, g_gate), 'rep')]
    pallas_call x0 -> x1, Pallas kernels: none -> 127 us  [on_device(): pl.pallas_call(functools.partial(kernel, sizes), out_shape=(jax.ShapeDtyp...]
    all_gather x2 -> x0, waiting for transfers between devices: 47.5 us -> none  [the longest x1 29.4 us: on_device(): whole_cot = lax.all_gather(cotangent[0], ('fs', 'tp'), axis=0, tiled=True)]
    reduce_scatter x1 -> x0, waiting for transfers between devices: 33.5 us -> none  [summed_rows(): own = lax.psum_scatter(everything, axis, scatter_dimension=0, tiled=True)]
    dot_general x6 -> x0, matrix products: 17.9 us -> none  [the longest x1 4.76 us: on_device(): jnp.dot(whole_cot, down_mat.T, preferred_element_type=jnp.float32)]
    psum x1 -> x0, blocking collectives: 12.4 us -> none  [weight_part(): g_taps, g_bias = lax.psum((g_taps, g_bias), 'rep')]
    mul x0 -> x3, local copies, waits for them, and re-layouts: none -> 3.81 us  [the longest x1 1.27 us: on_device(): g_down = parts[0].transpose(1, 0, 2).reshape(ff, width).astype(F32) * factor]
    unnamed x23 -> x13, local copies, waits for them, and re-layouts: 6.34 us -> 7.48 us
  transfers between devices with their start and end apart: 4 -> 0, of which waited for: 4 -> 0; matrix products, arithmetic and copies ran while one was open for 8% -> 0% of each run, Pallas kernels for 0% -> 0%
where the time goes in v1:
time: 146 us; the launch traced here: 145 us
  Pallas kernels  127 us (87%)
  local copies, waits for them, and re-layouts  13.8 us (9%)
  other arithmetic  2.64 us (2%)
    pallas_call x1, Pallas kernels, on_device(): pl.pallas_call(functools.partial(kernel, sizes), out_shape=(jax.ShapeDtyp...  127 us
    unnamed x13, local copies, waits for them, and re-layouts  7.48 us

profile of v1, /device:TPU:0, one launch (start us, length us, event | category | flops | bytes accessed | tf_op | source)
XLA Modules:
  0.0 144.6 jit_solution(2616649672408342130)
XLA Ops:
  0.6 0.0 copy-start.2
  0.6 1.3 broadcast_in_dim.6.bias_ref
  2.0 0.0 copy-start
  2.0 2.4 %copy.19 = bf16[1,1024,352]{2,1,0:T(8,128)(2,1)} copy(bf16[1,1024,352]{1,2,0:T(8,128)(2,1)} %param.10) | data formatting | bytes 1441792 | tf_op args[1]
  4.3 0.0 copy-done.2
  4.3 1.2 copy.20
  5.5 0.0 copy-done
  5.5 0.0 copy-start.1
  5.5 1.6 %copy.21.wup_hbm = f32[1024,352]{1,0:T(8,128)} copy(f32[1024,352]{0,1:T(8,128)S(1)} %copy-done) | data formatting | bytes 2883584 | tf_op args[4]
  7.1 0.0 copy-done.1
  7.1 1.6 %copy.22.wgate_hbm = f32[1024,352]{1,0:T(8,128)} copy(f32[1024,352]{0,1:T(8,128)S(1)} %copy-done.1) | data formatting | bytes 2883584 | tf_op args[5]
  8.7 127.5 %shard_map.136 = (bf16[128,1024]{1,0:T(8,128)(2,1)}, bf16[12,352,256]{2,1,0:T(8,128)(2,1)}, f32[8,352]{1,0:T(8,128)}) custom-call(bf16[128,1024]{1,0:T(8,128)(2,1)} %bitcast.22, bf16[128,1024]{1,0:T(8,128)(2,1)} %bitcast.23, f32[3,352]{1,0:T(4,128)} %taps_ref.1, f32[1,352]{1,0:T(1,128)} %broadcast_in_dim.6.bias_ref, bf16[1024,352]{1,0:T(8,128)(2,1)} %bitcast.17, ...), custom_call_target="tpu_custom_call" | custom-call | tf_op jit(solution)/shard_map/pallas_call | solution.py:502
  136.2 0.7 broadcast_multiply_fusion
  136.9 0.6 slice_reduce_fusion
  137.5 0.6 slice.23
  138.1 1.9 %multiply_bitcast_fusion = (f32[4,44,8,256]{3,2,1,0:T(8,128)S(1)}, f32[4,44,8,256]{3,2,1,0:T(8,128)S(1)}, f32[4,44,8,256]{3,2,1,0:T(8,128)S(1)}) fusion(bf16[12,352,256]{2,1,0:T(8,128)(2,1)} %get-tuple-element.10), kind=kLoop, calls=%fused_computation | loop fusion | flops 2162688 | bytes 6488064
  140.0 1.3 copy.28
  141.3 1.3 copy.27
  142.6 0.0 copy-start.3
  142.6 1.3 copy.26
  143.9 0.0 copy-done.3
  143.9 0.7 copy.30
Async XLA Ops:
  0.6 3.7 %copy-start.2 = (bf16[1,1024,352]{1,2,0:T(8,128)(2,1)S(1)}, bf16[1,1024,352]{1,2,0:T(8,128)(2,1)}, u32[]{:S(2)}) copy-start(bf16[1,1024,352]{1,2,0:T(8,128)(2,1)} %param.11) | copy-start | bytes 2162692
  2.0 3.5 %copy-start = (f32[1024,352]{0,1:T(8,128)S(1)}, f32[1024,352]{0,1:T(8,128)}, u32[]{:S(2)}) copy-start(f32[1024,352]{0,1:T(8,128)} %param.13) | copy-start | bytes 4325380
  5.5 1.6 %copy-start.1 = (f32[1024,352]{0,1:T(8,128)S(1)}, f32[1024,352]{0,1:T(8,128)}, u32[]{:S(2)}) copy-start(f32[1024,352]{0,1:T(8,128)} %param.14) | copy-start | bytes 4325380
  142.6 1.3 copy-start.3

commit v2 on v1

--- a/solution.py
+++ b/solution.py
@@ -13,10 +13,10 @@
 BF16 = jnp.bfloat16
 SLOPE = math.sqrt(2.0 / math.pi)
 CUBIC = 0.044715
-HALO = 8
 WIDE = 512
 CHUNK = 256
-ROWS = 128
+ROWS = 16
+LANES = 128
 
 
 def kernel(
@@ -32,7 +32,8 @@
     wgate_hbm,
     gi_ref,
     fin,
-    conv_out,
+    taps_out,
+    bias_out,
     cot_all,
     in_all,
     up_raw,
@@ -40,16 +41,17 @@
     wdown_f,
     wup_f,
     wgate_f,
-    up_pad,
     act,
     slope_gate,
     hid,
-    dconv,
+    d_hid,
     dgate,
     dup,
     down_b,
     up_b,
     gate_b,
+    in_rows,
+    in_cols,
     part,
     stage,
     conv_all,
@@ -73,9 +75,10 @@
     ring_rsem,
 ):
     n_rep, n_fs, n_tp = sizes
+    factor = float(n_rep * cot_all.shape[0]) ** (-0.5)
     me_r, me_f, me_c = lax.axis_index("rep"), lax.axis_index("fs"), lax.axis_index("tp")
     seq, width = cot_all.shape
-    ff = hid.shape[1]
+    ff = hid.shape[0]
     block = cot_ref.shape[0]
     taps = taps_ref.shape[0]
     per_grad = width // CHUNK
@@ -178,21 +181,27 @@
 
     pending = gather_sends(0, cot_ref, cot_all)
 
-    bias = bias_ref[...]
-    weight = [taps_ref[pl.ds(k, 1), :] for k in range(taps)]
-    up_pad[pl.ds(0, HALO), :] = jnp.zeros((HALO, ff), F32)
-    dconv[pl.ds(seq, HALO), :] = jnp.zeros((HALO, ff), F32)
+    in_rows[...] = jnp.zeros(in_rows.shape, F32)
+    in_rows[pl.ds(0, taps), pl.ds(0, ff)] = taps_ref[...]
+    in_rows[pl.ds(taps, 1), pl.ds(0, ff)] = bias_ref[...]
+    in_cols[...] = in_rows[...].T
+    lane = lax.broadcasted_iota(jnp.int32, (ROWS, seq), 1)
+
+    def later(value, k):
+        return value if k == 0 else jnp.where(lane >= k, pltpu.roll(value, k, 1), 0.0)
+
+    def sooner(value, k):
+        return value if k == 0 else jnp.where(lane < seq - k, pltpu.roll(value, seq - k, 1), 0.0)
+
     loads[0].wait()
     loads[1].wait()
 
     def forward(at, _):
         rows = pl.ds(pl.multiple_of(at * ROWS, ROWS), ROWS)
-        low = pl.multiple_of(at * ROWS, ROWS)
-        up_pad[pl.ds(pl.multiple_of(low + HALO, HALO), ROWS), :] = up_raw[rows, :].astype(F32)
-        ext = up_pad[pl.ds(low, ROWS + HALO), :]
-        total = bias + jnp.zeros((ROWS, ff), F32)
+        up = up_raw[rows, :].astype(F32)
+        total = in_cols[rows, taps : taps + 1] + jnp.zeros((ROWS, seq), F32)
         for k in range(taps):
-            total = total + weight[k] * ext[HALO - k : HALO - k + ROWS]
+            total = total + in_cols[rows, k : k + 1] * later(up, k)
         square = total * total
         bend = jnp.tanh(SLOPE * total * (1.0 + CUBIC * square))
         half = 0.5 * (1.0 + bend)
@@ -206,7 +215,7 @@
         slope_gate[rows, :] = slope * gate
         return 0
 
-    lax.fori_loop(0, seq // ROWS, forward, 0)
+    lax.fori_loop(0, ff // ROWS, forward, 0)
     loads[2].wait()
     down_b[...] = wdown_f[...].astype(BF16)
     loads[3].wait()
@@ -240,10 +249,13 @@
             stage.at[j], part.at[side, j], part_send.at[j], part_recv.at[side, j], {"rep": me_r}
         ).wait_recv()
 
+    def spot(j):
+        return j // per_grad, pl.ds(0, ff), pl.ds(j % per_grad * CHUNK, CHUNK)
+
     def final_copy(j, way):
         target = jnp.clip(me_r + (1 if way else -1), 0, n_rep - 1)
         return remote(
-            fin.at[j], fin.at[j], fin_send.at[way, j], fin_recv.at[j], {"rep": target}
+            fin.at[spot(j)], fin.at[spot(j)], fin_send.at[way, j], fin_recv.at[j], {"rep": target}
         )
 
     def is_edge(j):
@@ -274,7 +286,7 @@
             if o < n_rep - 1:
                 wait_part(1, j)
                 total = total + part[1, j].astype(F32)
-            fin[j] = total.astype(BF16)
+            fin[spot(j)] = total.astype(BF16)
             if o > 0:
                 final_copy(j, 0).start()
             if o < n_rep - 1:
@@ -300,11 +312,8 @@
 
     def weight_grad(grad, left, right):
         for piece in range(width // WIDE):
-            product = lax.dot_general(
-                left[...],
-                right[:, pl.ds(piece * WIDE, WIDE)],
-                over_rows,
-                preferred_element_type=F32,
+            product = jnp.dot(
+                left[...], right[:, pl.ds(piece * WIDE, WIDE)], preferred_element_type=F32
             ).astype(BF16)
             for sub in range(WIDE // CHUNK):
                 j = grad * per_grad + piece * (WIDE // CHUNK) + sub
@@ -313,42 +322,31 @@
 
     weight_grad(0, hid, cot_all)
 
-    def backward(at, sums):
-        low = pl.multiple_of(at * ROWS, ROWS)
-        rows = pl.ds(low, ROWS)
-        d_hidden = (
-            lax.dot_general(cot_all[rows, :], down_b[...], over_cols, preferred_element_type=F32)
-            .astype(BF16)
-            .astype(F32)
-        )
+    for piece in range(seq // WIDE):
+        cols = pl.ds(piece * WIDE, WIDE)
+        d_hid[:, cols] = lax.dot_general(
+            down_b[...], cot_all[cols, :], over_cols, preferred_element_type=F32
+        ).astype(BF16)
+    advance(0)
+
+    def backward(at, _):
+        rows = pl.ds(pl.multiple_of(at * ROWS, ROWS), ROWS)
+        d_hidden = d_hid[rows, :].astype(F32)
         dgate[rows, :] = (d_hidden * act[rows, :]).astype(BF16)
         d_conv = d_hidden * slope_gate[rows, :]
-        dconv[rows, :] = d_conv
-        ext = up_pad[pl.ds(low, ROWS + HALO), :]
-        new = [
-            sums[k]
-            + jnp.sum(d_conv * ext[HALO - k : HALO - k + ROWS], axis=0, keepdims=True)
-            for k in range(taps)
-        ]
-        return (*new, sums[taps] + jnp.sum(d_conv, axis=0, keepdims=True))
-
-    sums = lax.fori_loop(
-        0, seq // ROWS, backward, tuple(jnp.zeros((1, ff), F32) for _ in range(taps + 1))
-    )
-    conv_all[me_r] = jnp.zeros(conv_all.shape[1:], F32)
-    for k in range(taps + 1):
-        conv_all[me_r, pl.ds(k, 1), :] = sums[k]
-
-    def spread(at, _):
-        low = pl.multiple_of(at * ROWS, ROWS)
-        ext = dconv[pl.ds(low, ROWS + HALO), :]
-        total = weight[0] * ext[0:ROWS]
-        for k in range(1, taps):
-            total = total + weight[k] * ext[k : k + ROWS]
-        dup[pl.ds(low, ROWS), :] = total.astype(BF16)
+        up = up_raw[rows, :].astype(F32)
+        total = jnp.zeros((ROWS, seq), F32)
+        for k in range(taps):
+            ahead = sooner(d_conv, k)
+            total = total + in_cols[rows, k : k + 1] * ahead
+            in_cols[rows, taps + 1 + k : taps + 2 + k] = jnp.sum(ahead * up, axis=1, keepdims=True)
+        in_cols[rows, 2 * taps + 1 : 2 * taps + 2] = jnp.sum(d_conv, axis=1, keepdims=True)
+        dup[rows, :] = total.astype(BF16)
         return 0
 
-    lax.fori_loop(0, seq // ROWS, spread, 0)
+    lax.fori_loop(0, ff // ROWS, backward, 0)
+    in_rows[...] = in_cols[...].T
+    conv_all[me_r] = in_rows[pl.ds(0, 8), :]
 
     for step in range(1, n_rep):
         copy = remote(
@@ -361,7 +359,6 @@
         copy.start()
         pending.append(copy)
 
-    advance(0)
     pending += gather_finish(1, in_ref, in_all)
     weight_grad(1, dup, in_all)
     advance(1)
@@ -370,17 +367,17 @@
 
     def input_rows(core, store):
         left_up = jnp.concatenate(
-            [dup[rows_of(f * n_tp + core), :] for f in range(n_fs)], axis=0
+            [dup[:, rows_of(f * n_tp + core)] for f in range(n_fs)], axis=1
         )
         left_gate = jnp.concatenate(
-            [dgate[rows_of(f * n_tp + core), :] for f in range(n_fs)], axis=0
+            [dgate[:, rows_of(f * n_tp + core)] for f in range(n_fs)], axis=1
         )
         for piece in range(width // WIDE):
             cols = pl.ds(piece * WIDE, WIDE)
             total = lax.dot_general(
-                left_up, up_b[cols, :], over_cols, preferred_element_type=F32
+                left_up, up_b[:, cols], over_rows, preferred_element_type=F32
             ) + lax.dot_general(
-                left_gate, gate_b[cols, :], over_cols, preferred_element_type=F32
+                left_gate, gate_b[:, cols], over_rows, preferred_element_type=F32
             )
             store(cols, total)
 
@@ -462,7 +459,8 @@
     total = conv_all[0]
     for at in range(1, n_rep):
         total = total + conv_all[at]
-    conv_out[...] = total
+    taps_out[...] = total[taps + 1 : 2 * taps + 1, :ff] * factor
+    bias_out[...] = total[2 * taps + 1 : 2 * taps + 2, :ff] * factor
 
     for j in range(chunks - 2, chunks):
         deliver(j)
@@ -497,38 +495,40 @@
     devices = n_fs * n_tp
     vmem = pl.BlockSpec(memory_space=pltpu.VMEM)
     hbm = pl.BlockSpec(memory_space=pl.ANY)
-    conv_rows = -(-(taps + 1) // 8) * 8
     dma = pltpu.SemaphoreType.DMA
-    grad_inputs, fin, conv = pl.pallas_call(
+    padded = -(-ff // LANES) * LANES
+    grad_inputs, fin, g_taps, g_bias = pl.pallas_call(
         functools.partial(kernel, sizes),
         out_shape=(
             jax.ShapeDtypeStruct((block, width), BF16),
-            jax.ShapeDtypeStruct((chunks, ff, CHUNK), BF16),
-            jax.ShapeDtypeStruct((conv_rows, ff), F32),
+            jax.ShapeDtypeStruct((3, ff, width), BF16),
+            jax.ShapeDtypeStruct((taps, ff), F32),
+            jax.ShapeDtypeStruct((1, ff), F32),
         ),
         in_specs=[vmem] * 4 + [hbm] * 5,
-        out_specs=(vmem, vmem, vmem),
+        out_specs=(vmem,) * 4,
         scratch_shapes=[
             pltpu.VMEM((seq, width), BF16),
             pltpu.VMEM((seq, width), BF16),
-            pltpu.VMEM((seq, ff), BF16),
-            pltpu.VMEM((seq, ff), BF16),
+            pltpu.VMEM((ff, seq), BF16),
+            pltpu.VMEM((ff, seq), BF16),
             pltpu.VMEM((ff, width), F32),
-            pltpu.VMEM((width, ff), F32),
-            pltpu.VMEM((width, ff), F32),
-            pltpu.VMEM((seq + HALO, ff), F32),
-            pltpu.VMEM((seq, ff), F32),
-            pltpu.VMEM((seq, ff), F32),
-            pltpu.VMEM((seq, ff), BF16),
-            pltpu.VMEM((seq + HALO, ff), F32),
-            pltpu.VMEM((seq, ff), BF16),
-            pltpu.VMEM((seq, ff), BF16),
+            pltpu.VMEM((ff, width), F32),
+            pltpu.VMEM((ff, width), F32),
+            pltpu.VMEM((ff, seq), F32),
+            pltpu.VMEM((ff, seq), F32),
+            pltpu.VMEM((ff, seq), BF16),
+            pltpu.VMEM((ff, seq), BF16),
+            pltpu.VMEM((ff, seq), BF16),
+            pltpu.VMEM((ff, seq), BF16),
             pltpu.VMEM((ff, width), BF16),
-            pltpu.VMEM((width, ff), BF16),
-            pltpu.VMEM((width, ff), BF16),
+            pltpu.VMEM((ff, width), BF16),
+            pltpu.VMEM((ff, width), BF16),
+            pltpu.VMEM((LANES, padded), F32),
+            pltpu.VMEM((padded, LANES), F32),
             pltpu.VMEM((2, chunks, ff, CHUNK), BF16),
             pltpu.VMEM((chunks, ff, CHUNK), BF16),
-            pltpu.VMEM((n_rep, conv_rows, ff), F32),
+            pltpu.VMEM((n_rep, 8, padded), F32),
             pltpu.VMEM((n_tp - 1, n_fs * block, width), BF16),
             pltpu.VMEM((n_tp - 1, n_fs * block, width), BF16),
             pltpu.VMEM((n_fs * block, width), F32),
@@ -556,19 +556,16 @@
         inputs[0],
         conv_weight,
         conv_bias[None],
-        up_pre[0],
-        gate_pre[0],
+        up_pre[0].T,
+        gate_pre[0].T,
         w_down,
-        w_up,
-        w_gate,
+        w_up.T,
+        w_gate.T,
     )
-    per_grad = width // CHUNK
-    parts = fin.reshape(3, per_grad, ff, CHUNK)
-    g_down = parts[0].transpose(1, 0, 2).reshape(ff, width).astype(F32) * factor
-    g_up = parts[1].transpose(0, 2, 1).reshape(width, ff).astype(F32) * factor
-    g_gate = parts[2].transpose(0, 2, 1).reshape(width, ff).astype(F32) * factor
-    conv = conv * factor
-    return grad_inputs[None], g_up, g_gate, g_down, conv[:taps], conv[taps]
+    g_down = fin[0].astype(F32) * factor
+    g_up = fin[1].T.astype(F32) * factor
+    g_gate = fin[2].T.astype(F32) * factor
+    return grad_inputs[None], g_up, g_gate, g_down, g_taps, g_bias[0]
 
 
 def solution(mesh):

time: 146 us -> 143 us (0.979)
  local copies, waits for them, and re-layouts: 13.8 us -> 2.55 us
  Pallas kernels: 127 us -> 133 us
  other arithmetic: 2.64 us -> 4.4 us
    unnamed x13 -> x8, local copies, waits for them, and re-layouts: 7.48 us -> 1.31 us
    pallas_call x1, Pallas kernels: 127 us -> 133 us  [on_device(): pl.pallas_call(functools.partial(kernel, sizes), out_shape=(jax.ShapeDtyp...]
    mul x3 -> x0, local copies, waits for them, and re-layouts: 3.81 us -> none  [the longest x1 1.27 us: on_device(): g_down = parts[0].transpose(1, 0, 2).reshape(ff, width).astype(F32) * factor]
    mul x1, other arithmetic: 0.71 us -> 3.8 us  [on_device(): g_down = fin[0].astype(F32) * factor]
    unnamed x1 -> x0, other arithmetic: 1.93 us -> none
where the time goes in v2:
time: 143 us; the launch traced here: 141 us
  Pallas kernels  133 us (93%)
  other arithmetic  4.4 us (3%)
  local copies, waits for them, and re-layouts  2.55 us (2%)
    pallas_call x1, Pallas kernels, on_device(): pl.pallas_call(functools.partial(kernel, sizes), out_shape=(jax.ShapeDtyp...  133 us
    mul x1, other arithmetic, on_device(): g_down = fin[0].astype(F32) * factor  3.8 us

profile of v2, /device:TPU:0, one launch (start us, length us, event | category | flops | bytes accessed | tf_op | source)
XLA Modules:
  0.0 140.6 jit_solution(4615172772340595051)
XLA Ops:
  0.6 1.2 broadcast_in_dim.6.bias_ref
  1.9 132.9 %shard_map.136 = (bf16[128,1024]{1,0:T(8,128)(2,1)}, bf16[3,352,1024]{2,1,0:T(8,128)(2,1)}, f32[3,352]{1,0:T(4,128)}, f32[1,352]{1,0:T(1,128)}) custom-call(bf16[128,1024]{1,0:T(8,128)(2,1)} %bitcast.25, bf16[128,1024]{1,0:T(8,128)(2,1)} %bitcast.26, f32[3,352]{1,0:T(4,128)} %taps_ref.1, f32[1,352]{1,0:T(1,128)} %broadcast_in_dim.6.bias_ref, ...), custom_call_target="tpu_custom_call" | custom-call | tf_op jit(solution)/shard_map/pallas_call | solution.py:500
  134.8 0.0 copy-start.2
  134.8 0.0 copy-start
  134.8 0.0 copy-start.1
  134.9 3.8 %multiply_bitcast_fusion = (f32[352,1024]{1,0:T(8,128)}, f32[1024,352]{0,1:T(8,128)}, f32[1024,352]{0,1:T(8,128)}) fusion(bf16[3,352,1024]{2,1,0:T(8,128)(2,1)} %get-tuple-element.11), kind=kLoop, calls=%fused_computation | loop fusion | flops 2162688 | bytes 6488064 | tf_op jit(solution)/shard_map/mul | solution.py:565
  138.7 0.0 copy-done.2
  138.7 0.6 reduce
  139.3 0.0 copy-done
  139.3 0.7 copy.17
  140.0 0.0 copy-done.1
  140.0 0.6 copy.18
Async XLA Ops:
  134.8 3.8 %copy-start.2 = (f32[1,352]{1,0:T(1,128)S(1)}, f32[1,352]{1,0:T(1,128)}, u32[]{:S(2)}) copy-start(f32[1,352]{1,0:T(1,128)} %get-tuple-element.13) | copy-start | bytes 4228
  134.8 4.4 %copy-start = (bf16[128,1024]{1,0:T(8,128)(2,1)S(1)}, bf16[128,1024]{1,0:T(8,128)(2,1)}, u32[]{:S(2)}) copy-start(bf16[128,1024]{1,0:T(8,128)(2,1)} %get-tuple-element.10) | copy-start | bytes 786436
  134.8 5.1 %copy-start.1 = (f32[3,352]{1,0:T(4,128)S(1)}, f32[3,352]{1,0:T(4,128)}, u32[]{:S(2)}) copy-start(f32[3,352]{1,0:T(4,128)} %get-tuple-element.27) | copy-start | bytes 12676

commit v3 on v2

--- a/solution.py
+++ b/solution.py
@@ -15,6 +15,9 @@
 CUBIC = 0.044715
 WIDE = 512
 CHUNK = 256
+FLIGHT = 2
+OWN_LAG = 2
+LAG = 5
 ROWS = 16
 LANES = 128
 
@@ -54,6 +57,7 @@
     in_cols,
     part,
     stage,
+    land,
     conv_all,
     pair_send,
     pair_recv,
@@ -255,7 +259,7 @@
     def final_copy(j, way):
         target = jnp.clip(me_r + (1 if way else -1), 0, n_rep - 1)
         return remote(
-            fin.at[spot(j)], fin.at[spot(j)], fin_send.at[way, j], fin_recv.at[j], {"rep": target}
+            land.at[j], land.at[j], fin_send.at[way, j], fin_recv.at[j], {"rep": target}
         )
 
     def is_edge(j):
@@ -266,8 +270,15 @@
         def _():
             partial_copy(j).start()
 
-    def advance(j):
+    def pass_on(j):
         o = owner_of(j)
+        if j + FLIGHT < chunks:
+
+            @pl.when(is_edge(j))
+            def _():
+                partial_copy(j).wait_send()
+                partial_copy(j + FLIGHT).start()
+
         for side in (0, 1):
             inner = (me_r < o) if side == 0 else (me_r > o)
 
@@ -276,6 +287,9 @@
                 wait_part(side, j)
                 stage[j] = (stage[j].astype(F32) + part[side, j].astype(F32)).astype(BF16)
                 partial_copy(j).start()
+
+    def own_sum(j):
+        o = owner_of(j)
 
         @pl.when(me_r == o)
         def _():
@@ -286,7 +300,7 @@
             if o < n_rep - 1:
                 wait_part(1, j)
                 total = total + part[1, j].astype(F32)
-            fin[spot(j)] = total.astype(BF16)
+            land[j] = total.astype(BF16)
             if o > 0:
                 final_copy(j, 0).start()
             if o < n_rep - 1:
@@ -306,6 +320,18 @@
         @pl.when(jnp.logical_and(me_r > o, me_r < n_rep - 1))
         def _():
             final_copy(j, 1).start()
+
+    def settle(j):
+        deliver(j)
+        fin[spot(j)] = land[j]
+
+    def advance(k):
+        if k < chunks:
+            pass_on(k)
+        if 0 <= k - OWN_LAG < chunks:
+            own_sum(k - OWN_LAG)
+        if 0 <= k - LAG < chunks:
+            settle(k - LAG)
 
     over_rows = (((0,), (0,)), ((), ()))
     over_cols = (((1,), (1,)), ((), ()))
@@ -318,7 +344,8 @@
             for sub in range(WIDE // CHUNK):
                 j = grad * per_grad + piece * (WIDE // CHUNK) + sub
                 stage[j] = product[:, sub * CHUNK : (sub + 1) * CHUNK]
-                start_edge(j)
+                if j < FLIGHT:
+                    start_edge(j)
 
     weight_grad(0, hid, cot_all)
 
@@ -396,7 +423,6 @@
         )
         copy.start()
         pending.append(copy)
-    deliver(0)
     advance(3)
 
     def store_keep(cols, total):
@@ -427,10 +453,8 @@
         )
         copy.start()
         pending.append(copy)
-    deliver(1)
     for j in range(4, chunks):
         advance(j)
-        deliver(j - 2)
 
     own = rows_of(me_f)
     total = keep[own, :]
@@ -462,15 +486,19 @@
     taps_out[...] = total[taps + 1 : 2 * taps + 1, :ff] * factor
     bias_out[...] = total[2 * taps + 1 : 2 * taps + 2, :ff] * factor
 
-    for j in range(chunks - 2, chunks):
-        deliver(j)
+    for j in range(chunks, chunks + LAG):
+        advance(j)
 
     for copy in pending:
         copy.wait_send()
     for j in range(chunks):
         o = owner_of(j)
 
-        @pl.when(me_r != o)
+        unsent = me_r != o
+        if j + FLIGHT < chunks:
+            unsent = jnp.logical_and(unsent, has_away(j))
+
+        @pl.when(unsent)
         def _():
             partial_copy(j).wait_send()
 
@@ -528,6 +556,7 @@
             pltpu.VMEM((padded, LANES), F32),
             pltpu.VMEM((2, chunks, ff, CHUNK), BF16),
             pltpu.VMEM((chunks, ff, CHUNK), BF16),
+            pltpu.VMEM((chunks, ff, CHUNK), BF16),
             pltpu.VMEM((n_rep, 8, padded), F32),
             pltpu.VMEM((n_tp - 1, n_fs * block, width), BF16),
             pltpu.VMEM((n_tp - 1, n_fs * block, width), BF16),

time: 143 us -> 102 us (0.71); the launches traced: 141 us -> 102 us
  Pallas kernels: 133 us -> 94.3 us
    pallas_call x1, Pallas kernels: 133 us -> 94.3 us  [on_device(): pl.pallas_call(functools.partial(kernel, sizes), out_shape=(jax.ShapeDtyp...]
where the time goes in v3:
time: 102 us
  Pallas kernels  94.3 us (92%)
  other arithmetic  4.4 us (4%)
  local copies, waits for them, and re-layouts  2.55 us (2%)
    pallas_call x1, Pallas kernels, on_device(): pl.pallas_call(functools.partial(kernel, sizes), out_shape=(jax.ShapeDtyp...  94.3 us
    mul x1, other arithmetic, on_device(): g_down = fin[0].astype(F32) * factor  3.8 us

profile of v3, /device:TPU:0, one launch (start us, length us, event | category | flops | bytes accessed | tf_op | source)
XLA Modules:
  0.0 101.9 jit_solution(9711850752926472677)
XLA Ops:
  0.6 1.2 %broadcast_in_dim.6.bias_ref = f32[1,352]{1,0:T(1,128)} reshape(f32[352]{0:T(512)} %param.17) | data formatting | bytes 2816 | tf_op jit(solution)/shard_map/broadcast_in_dim | solution.py:587
  1.9 94.3 %shard_map.136 = (bf16[128,1024]{1,0:T(8,128)(2,1)}, bf16[3,352,1024]{2,1,0:T(8,128)(2,1)}, f32[3,352]{1,0:T(4,128)}, f32[1,352]{1,0:T(1,128)}) custom-call(bf16[128,1024]{1,0:T(8,128)(2,1)} %bitcast.25, bf16[128,1024]{1,0:T(8,128)(2,1)} %bitcast.26, f32[3,352]{1,0:T(4,128)} %taps_ref.1, f32[1,352]{1,0:T(1,128)} %broadcast_in_dim.6.bias_ref, ...), custom_call_target="tpu_custom_call" | custom-call | tf_op jit(solution)/shard_map/pallas_call | solution.py:528
  96.2 0.0 copy-start.2
  96.2 0.0 copy-start
  96.2 0.0 copy-start.1
  96.2 3.8 %multiply_bitcast_fusion = (f32[352,1024]{1,0:T(8,128)}, f32[1024,352]{0,1:T(8,128)}, f32[1024,352]{0,1:T(8,128)}) fusion(bf16[3,352,1024]{2,1,0:T(8,128)(2,1)} %get-tuple-element.11), kind=kLoop, calls=%fused_computation | loop fusion | flops 2162688 | bytes 6488064 | tf_op jit(solution)/shard_map/mul | solution.py:594
  100.0 0.0 copy-done.2
  100.0 0.6 reduce
  100.6 0.0 copy-done
  100.6 0.7 copy.17
  101.3 0.0 copy-done.1
  101.4 0.6 copy.18
Async XLA Ops:
  96.2 3.8 %copy-start.2 = (f32[1,352]{1,0:T(1,128)S(1)}, f32[1,352]{1,0:T(1,128)}, u32[]{:S(2)}) copy-start(f32[1,352]{1,0:T(1,128)} %get-tuple-element.13) | copy-start | bytes 4228
  96.2 4.4 %copy-start = (bf16[128,1024]{1,0:T(8,128)(2,1)S(1)}, bf16[128,1024]{1,0:T(8,128)(2,1)}, u32[]{:S(2)}) copy-start(bf16[128,1024]{1,0:T(8,128)(2,1)} %get-tuple-element.10) | copy-start | bytes 786436
  96.2 5.1 %copy-start.1 = (f32[3,352]{1,0:T(4,128)S(1)}, f32[3,352]{1,0:T(4,128)}, u32[]{:S(2)}) copy-start(f32[3,352]{1,0:T(4,128)} %get-tuple-element.27) | copy-start | bytes 12676

commit v4 on v3

--- a/solution.py
+++ b/solution.py
@@ -15,7 +15,7 @@
 CUBIC = 0.044715
 WIDE = 512
 CHUNK = 256
-FLIGHT = 2
+FLIGHT = 4
 OWN_LAG = 2
 LAG = 5
 ROWS = 16
@@ -270,8 +270,7 @@
         def _():
             partial_copy(j).start()
 
-    def pass_on(j):
-        o = owner_of(j)
+    def refill(j):
         if j + FLIGHT < chunks:
 
             @pl.when(is_edge(j))
@@ -279,6 +278,8 @@
                 partial_copy(j).wait_send()
                 partial_copy(j + FLIGHT).start()
 
+    def pass_on(j):
+        o = owner_of(j)
         for side in (0, 1):
             inner = (me_r < o) if side == 0 else (me_r > o)
 
@@ -325,8 +326,10 @@
         deliver(j)
         fin[spot(j)] = land[j]
 
-    def advance(k):
+    def advance(k, fill=True):
         if k < chunks:
+            if fill:
+                refill(k)
             pass_on(k)
         if 0 <= k - OWN_LAG < chunks:
             own_sum(k - OWN_LAG)
@@ -354,7 +357,7 @@
         d_hid[:, cols] = lax.dot_general(
             down_b[...], cot_all[cols, :], over_cols, preferred_element_type=F32
         ).astype(BF16)
-    advance(0)
+    advance(0, False)
 
     def backward(at, _):
         rows = pl.ds(pl.multiple_of(at * ROWS, ROWS), ROWS)
@@ -386,11 +389,14 @@
         copy.start()
         pending.append(copy)
 
+    advance(1, False)
     pending += gather_finish(1, in_ref, in_all)
     weight_grad(1, dup, in_all)
-    advance(1)
+    for j in range(2):
+        refill(j)
+    advance(2)
     weight_grad(2, dgate, in_all)
-    advance(2)
+    advance(3)
 
     def input_rows(core, store):
         left_up = jnp.concatenate(
@@ -423,7 +429,7 @@
         )
         copy.start()
         pending.append(copy)
-    advance(3)
+    advance(4)
 
     def store_keep(cols, total):
         keep[:, cols] = total
@@ -453,7 +459,7 @@
         )
         copy.start()
         pending.append(copy)
-    for j in range(4, chunks):
+    for j in range(5, chunks):
         advance(j)
 
     own = rows_of(me_f)

time: 102 us -> 101 us (level)
  no operation moved by 1% of the time
where the time goes in v4:
time: 101 us
  Pallas kernels  93.4 us (92%)
  other arithmetic  4.4 us (4%)
  local copies, waits for them, and re-layouts  2.55 us (3%)
    pallas_call x1, Pallas kernels, on_device(): pl.pallas_call(functools.partial(kernel, sizes), out_shape=(jax.ShapeDtyp...  93.4 us
    mul x1, other arithmetic, on_device(): g_down = fin[0].astype(F32) * factor  3.8 us

profile of v4, /device:TPU:0, one launch (start us, length us, event | category | flops | bytes accessed | tf_op | source)
XLA Modules:
  0.0 101.0 jit_solution(16388101201409903022)
XLA Ops:
  0.6 1.2 %broadcast_in_dim.6.bias_ref = f32[1,352]{1,0:T(1,128)} reshape(f32[352]{0:T(512)} %param.17) | data formatting | bytes 2816 | tf_op jit(solution)/shard_map/broadcast_in_dim | solution.py:593
  1.9 93.4 %shard_map.136 = (bf16[128,1024]{1,0:T(8,128)(2,1)}, bf16[3,352,1024]{2,1,0:T(8,128)(2,1)}, f32[3,352]{1,0:T(4,128)}, f32[1,352]{1,0:T(1,128)}) custom-call(bf16[128,1024]{1,0:T(8,128)(2,1)} %bitcast.25, bf16[128,1024]{1,0:T(8,128)(2,1)} %bitcast.26, f32[3,352]{1,0:T(4,128)} %taps_ref.1, f32[1,352]{1,0:T(1,128)} %broadcast_in_dim.6.bias_ref, ...), custom_call_target="tpu_custom_call" | custom-call | tf_op jit(solution)/shard_map/pallas_call | solution.py:534
  95.3 0.0 copy-start.2
  95.3 0.0 copy-start
  95.3 0.0 copy-start.1
  95.3 3.8 %multiply_bitcast_fusion = (f32[352,1024]{1,0:T(8,128)}, f32[1024,352]{0,1:T(8,128)}, f32[1024,352]{0,1:T(8,128)}) fusion(bf16[3,352,1024]{2,1,0:T(8,128)(2,1)} %get-tuple-element.11), kind=kLoop, calls=%fused_computation | loop fusion | flops 2162688 | bytes 6488064 | tf_op jit(solution)/shard_map/mul | solution.py:600
  99.1 0.0 copy-done.2
  99.1 0.6 reduce
  99.7 0.0 copy-done
  99.7 0.7 copy.17
  100.4 0.0 copy-done.1
  100.4 0.6 copy.18
Async XLA Ops:
  95.3 3.8 %copy-start.2 = (f32[1,352]{1,0:T(1,128)S(1)}, f32[1,352]{1,0:T(1,128)}, u32[]{:S(2)}) copy-start(f32[1,352]{1,0:T(1,128)} %get-tuple-element.13) | copy-start | bytes 4228
  95.3 4.4 %copy-start = (bf16[128,1024]{1,0:T(8,128)(2,1)S(1)}, bf16[128,1024]{1,0:T(8,128)(2,1)}, u32[]{:S(2)}) copy-start(bf16[128,1024]{1,0:T(8,128)(2,1)} %get-tuple-element.10) | copy-start | bytes 786436
  95.3 5.1 %copy-start.1 = (f32[3,352]{1,0:T(4,128)S(1)}, f32[3,352]{1,0:T(4,128)}, u32[]{:S(2)}) copy-start(f32[3,352]{1,0:T(4,128)} %get-tuple-element.27) | copy-start | bytes 12676
